TPU v7x, 32 devices: a whole 2x2x4 slice. The times are simulated.
32 devices in a mesh: grp: 2 (over y), ep: 8 (over z, x), tp: 2 (over core).
Axes of the slice: x: 2, y: 2, z: 4, core: 2. Of those that a mesh axis runs over, the one named last changes fastest.
Arguments:
- tokens: bfloat16 [4096, 2048], P(('grp', 'ep', 'tp')), parts along dimension 0, may hold values from -6 to 6
- norm_gain: float32 [2048], replicated, may hold values from 0.1 to 1.9
- expert_ids: int32 [4096, 2], P(('grp', 'ep', 'tp')), parts along dimension 0, may hold values from 0 to 3, all different within a row; in each aligned block of 128 rows (0 to 127, 128 to 255, ...) at most 80 rows name the same one
- route_weights: float32 [4096, 2], P(('grp', 'ep', 'tp')), parts along dimension 0, may hold values from 0.1 to 0.9
- w_gate: bfloat16 [2048, 14336], P(None, ('ep', 'tp')), may hold values from -0.125 to 0.125
- w_up: bfloat16 [2048, 14336], P(None, ('ep', 'tp')), may hold values from -0.125 to 0.125
- w_down: bfloat16 [14336, 2048], P(('ep', 'tp')), may hold values from -0.09375 to 0.09375
Outputs:
- mixed_out: bfloat16 [4096, 2048], P(('grp', 'ep', 'tp')), parts along dimension 0
There are 2 independent parts, one for each index of `grp`. A program takes and returns all parts, laid end to end along the dimension named above; an argument that names none is the same for every part. Nothing has to cross between parts.
Inputs may be any that keep to these rules, and one draw needn't show every extreme that they name: `expert_ids`: each row names 2 different experts. Among the rows of one device no expert is named more than 80 times, and in every draw some expert is named exactly 80 times by one device's rows.
All inputs are finite; a program needn't handle non-finite values.
Results may differ from a plain program's by a relative error of at most 0.01.
Values may be sent and summed in bfloat16 or wider, within the bound.
A program may use at most 128 MiB of HBM per device.

v0:
```python
import functools

import jax
import jax.numpy as jnp
from jax import lax
from jax.experimental import pallas as pl
from jax.experimental.pallas import tpu as pltpu
from jax.sharding import PartitionSpec as P

MESH = pl.DeviceIdType.MESH
LANE = 128
PIECES = 2


def turn(i, experts):
    return i % experts


def mix_index(first, second, count):
    total = first * 0
    bit = 1
    while bit < count:
        one, two = (first // bit) % 2, (second // bit) % 2
        total = total + bit * (one + two - 2 * one * two)
        bit *= 2
    return total


def kernel(
    experts, cap,
    tok_ref, gain_ref, ids_ref, weight_ref, gate_ref, up_ref, down_ref,
    out_ref,
    norm, xs, xa, hid, po, rd, cx, rx, fo, ret, wgu, wd,
    gate_sem, up_sem, down_sem, own_sem,
    z_send, z_recv, x_send, x_recv, d_send, d_recv, e_send, e_recv,
    r_send, r_recv, v_send, v_recv, w_send, w_recv,
):
    ep, c = lax.axis_index("ep"), lax.axis_index("tp")
    p, h = ep // 2, ep % 2
    toks, width = tok_ref.shape
    tiles = wgu.shape[0]
    part_width = width // PIECES
    across = {"ep": 2 * p + 1 - h, "tp": c}
    beside = {"ep": ep, "tp": 1 - c}

    def plane(q):
        return {"ep": 2 * q + h, "tp": c}

    barrier = pltpu.get_barrier_semaphore()

    def greet(k, carry):
        pl.semaphore_signal(barrier, inc=1, device_id=plane(mix_index(p, k, experts)), device_id_type=MESH)
        return carry

    lax.fori_loop(1, experts, greet, 0)
    pl.semaphore_signal(barrier, inc=1, device_id=across, device_id_type=MESH)
    pl.semaphore_signal(barrier, inc=1, device_id=beside, device_id_type=MESH)

    def gate_copy(j):
        return pltpu.make_async_copy(
            gate_ref.at[:, pl.ds(j * LANE, LANE)], wgu.at[j, :, pl.ds(0, LANE)], gate_sem.at[j])

    def up_copy(j):
        return pltpu.make_async_copy(
            up_ref.at[:, pl.ds(j * LANE, LANE)], wgu.at[j, :, pl.ds(LANE, LANE)], up_sem.at[j])

    down_copy = pltpu.make_async_copy(down_ref, wd, down_sem)
    for j in range(tiles):
        gate_copy(j).start()
        up_copy(j).start()
    down_copy.start()

    values = tok_ref[...].astype(jnp.float32)
    scale_rows = lax.rsqrt(jnp.mean(values * values, axis=1, keepdims=True) + 1e-06)
    norm[...] = (values * scale_rows * gain_ref[...]).astype(jnp.bfloat16)

    row = lax.broadcasted_iota(jnp.int32, (toks, toks), 0)
    col = lax.broadcasted_iota(jnp.int32, (toks, toks), 1)
    before = (row < col).astype(jnp.float32).astype(jnp.bfloat16)
    slots = lax.broadcasted_iota(jnp.int32, (cap, toks), 0).astype(jnp.float32)

    def remote(src, dst, send, recv, target):
        return pltpu.make_async_remote_copy(
            src_ref=src, dst_ref=dst, send_sem=send, recv_sem=recv, device_id=target, device_id_type=MESH)

    def cut(ref, index, g):
        return ref.at[index, :, pl.ds(g * part_width, part_width)]

    def z_pair(k, g, origin):
        q = mix_index(p, k, experts)
        n = PIECES * k + g
        return remote(
            cut(xs, q, g), cut(xa, 4 * origin(q) + 2 * h + c, g), z_send.at[n], z_recv.at[n], plane(q))

    def z_copy(k, g):
        return z_pair(k, g, lambda q: p)

    def z_land(k, g):
        return z_pair(k, g, lambda q: q)

    own_copy = pltpu.make_async_copy(xs.at[p], xa.at[4 * p + 2 * h + c], own_sem)

    def mine(k, half, core, g):
        return cut(xa, 4 * mix_index(p, k, experts) + 2 * half + core, g)

    def shift(k, g, there, here, send, recv, target):
        n = PIECES * k + g
        return remote(mine(k, *there, g), mine(k, *here, g), send.at[n], recv.at[n], target)

    def x_copy(k, g):
        return shift(k, g, (h, c), (h, c), x_send, x_recv, across)

    def x_land(k, g):
        return shift(k, g, (h, c), (1 - h, c), x_send, x_recv, across)

    def d_copy(k, g):
        return shift(k, g, (h, c), (h, c), d_send, d_recv, beside)

    def d_land(k, g):
        return shift(k, g, (h, c), (h, 1 - c), d_send, d_recv, beside)

    def e_copy(k, g):
        return shift(k, g, (1 - h, c), (1 - h, c), e_send, e_recv, beside)

    def e_land(k, g):
        return shift(k, g, (1 - h, c), (1 - h, 1 - c), e_send, e_recv, beside)

    def r_copy(k, half, g):
        n = 2 * (PIECES * k + g) + half
        return remote(
            cut(po, 4 * k + 2 * half + 1 - c, g), cut(rd, 2 * k + half, g),
            r_send.at[n], r_recv.at[n], beside)

    def v_copy(k, g):
        n = PIECES * k + g
        return remote(cut(cx, 2 * k + 1 - h, g), cut(rx, k, g), v_send.at[n], v_recv.at[n], across)

    def w_pair(k, g, origin):
        q = mix_index(p, k, experts)
        n = PIECES * k + g
        return remote(cut(fo, k, g), cut(ret, origin(q), g), w_send.at[n], w_recv.at[n], plane(q))

    def w_copy(k, g):
        return w_pair(k, g, lambda q: p)

    def w_land(k, g):
        return w_pair(k, g, lambda q: q)

    pl.semaphore_wait(barrier, experts + 1)

    def fill(i, carry):
        k = turn(i + 1, experts)
        e = mix_index(p, k, experts)
        named = ((ids_ref[0:1, :] == e) | (ids_ref[1:2, :] == e)).astype(jnp.float32)
        rank = jnp.dot(
            jnp.broadcast_to(named, (16, toks)).astype(jnp.bfloat16), before,
            preferred_element_type=jnp.float32)[0:1, :]
        pick = jnp.where(slots == rank, named, 0.0).astype(jnp.bfloat16)
        xs[e] = jnp.dot(pick, norm[...], preferred_element_type=jnp.float32).astype(jnp.bfloat16)

        @pl.when(k > 0)
        def _():
            for g in range(PIECES):
                z_copy(k, g).start()

        return carry

    lax.fori_loop(0, experts, fill, 0)
    own_copy.start()
    own_copy.wait()

    step = 2 * LANE

    def compute(k):
        first = 4 * mix_index(p, k, experts)

        def gate_up(j, carry):
            rows = xa[pl.ds(first, 4)].reshape(4 * cap, width)
            both = jnp.dot(rows, wgu[j], preferred_element_type=jnp.float32)
            gate, up = both[:, :LANE], both[:, LANE:]
            hid[:, pl.ds(pl.multiple_of(j * LANE, LANE), LANE)] = (
                gate / (1.0 + jnp.exp(-gate)) * up).astype(jnp.bfloat16)
            return carry

        lax.fori_loop(0, tiles, gate_up, 0)

        def down(n, carry):
            place = pl.ds(pl.multiple_of(n * step, step), step)
            part = jnp.dot(hid[...], wd[:, place], preferred_element_type=jnp.float32)
            po[pl.ds(4 * k, 4), :, place] = part.astype(jnp.bfloat16).reshape(4, cap, step)
            return carry

        many = part_width // step
        for g in range(PIECES):
            lax.fori_loop(g * many, (g + 1) * many, down, 0)
            for half in range(2):
                r_copy(k, half, g).start()

    def add(first, second):
        return (first.astype(jnp.float32) + second.astype(jnp.float32)).astype(jnp.bfloat16)

    def finish(k):
        for g in range(PIECES):
            v_copy(k, g).wait_recv()
            cols = pl.ds(g * part_width, part_width)
            total = add(cx[2 * k + h, :, cols], rx[k, :, cols])

            @pl.when(k == 0)
            def _():
                ret[p, :, cols] = total

            @pl.when(k > 0)
            def _():
                fo[k, :, cols] = total
                w_copy(k, g).start()

    def stage(i, carry):
        @pl.when(i < experts)
        def _():
            k = turn(i, experts)
            for g in range(PIECES):
                @pl.when(k > 0)
                def _():
                    z_land(k, g).wait_recv()

                x_copy(k, g).start()
                d_copy(k, g).start()

        @pl.when(i > 0)
        def _():
            k = turn(i - 1, experts)
            for g in range(PIECES):
                x_land(k, g).wait_recv()
                e_copy(k, g).start()

            @pl.when(i == 1)
            def _():
                for j in range(tiles):
                    gate_copy(j).wait()
                    up_copy(j).wait()
                down_copy.wait()

            for g in range(PIECES):
                d_land(k, g).wait_recv()
                e_land(k, g).wait_recv()
            compute(k)

            @pl.when(i > 2)
            def _():
                finish(turn(i - 2, experts))

            for g in range(PIECES):
                cols = pl.ds(g * part_width, part_width)
                for half in range(2):
                    r_copy(k, half, g).wait_recv()
                    cx[2 * k + half, :, cols] = add(
                        po[4 * k + 2 * half + c, :, cols], rd[2 * k + half, :, cols])

                @pl.when(k > 0)
                def _():
                    v_copy(k, g).start()

        return carry

    lax.fori_loop(0, experts + 1, stage, 0)
    for g in range(PIECES):
        v_copy(0, g).start()

    def settle(k, carry):
        for g in range(PIECES):
            x_copy(k, g).wait_send()
            d_copy(k, g).wait_send()
            e_copy(k, g).wait_send()
            r_copy(k, 0, g).wait_send()
            r_copy(k, 1, g).wait_send()
            v_copy(k, g).wait_send()

            @pl.when(k > 0)
            def _():
                z_copy(k, g).wait_send()
                w_copy(k, g).wait_send()

        return carry

    after = (col < row).astype(jnp.float32).astype(jnp.bfloat16)

    sides = jnp.concatenate(
        [ids_ref[...].astype(jnp.float32), weight_ref[...], jnp.zeros((LANE - 4, toks), jnp.float32)], axis=0).T

    def place_of(e, places):
        number = lax.convert_element_type(e, jnp.float32)
        hits = [(sides[:, n:n + 1] == number).astype(jnp.float32) for n in range(2)]
        rank = jnp.dot(
            after, jnp.broadcast_to(hits[0] + hits[1], (toks, LANE)).astype(jnp.bfloat16),
            preferred_element_type=jnp.float32)[:, 0:1]
        spot = rank + number * cap
        return tuple(old + hit * spot for old, hit in zip(places, hits))

    zero = jnp.zeros((toks, 1), jnp.float32)
    places = lax.fori_loop(0, experts, place_of, (zero, zero))
    lanes = lax.broadcasted_iota(jnp.int32, (toks, experts * cap), 1).astype(jnp.float32)
    picks = [(lanes == place).astype(jnp.float32).astype(jnp.bfloat16) for place in places]
    finish(turn(experts - 1, experts))
    finish(0)
    lax.fori_loop(0, experts, settle, 0)
    for g in range(PIECES):
        def landed(k, carry):
            w_land(k, g).wait_recv()
            return carry

        lax.fori_loop(1, experts, landed, 0)
        cols = pl.ds(g * part_width, part_width)
        rows = ret[:, :, cols].reshape(experts * cap, part_width)
        total = jnp.zeros((toks, part_width), jnp.float32)
        for m in range(2):
            total = total + sides[:, 2 + m:3 + m] * jnp.dot(
                picks[m], rows, preferred_element_type=jnp.float32)
        out_ref[:, cols] = total.astype(jnp.bfloat16)


def local(tokens, norm_gain, expert_ids, route_weights, w_gate, w_up, w_down):
    experts = lax.axis_size("ep") // 2
    toks, width = tokens.shape
    hidden = w_gate.shape[1]
    capacity = 2 * max(1, 5 * toks * expert_ids.shape[1] // (8 * experts))
    cap = -(-capacity // 16) * 16
    tiles = hidden // LANE
    vmem, any_space = pl.BlockSpec(memory_space=pltpu.VMEM), pl.BlockSpec(memory_space=pl.ANY)
    dma = pltpu.SemaphoreType.DMA
    bf16 = jnp.bfloat16
    return pl.pallas_call(
        functools.partial(kernel, experts, cap),
        out_shape=jax.ShapeDtypeStruct((toks, width), bf16),
        in_specs=[vmem] * 4 + [any_space] * 3,
        out_specs=vmem,
        scratch_shapes=[
            pltpu.VMEM((toks, width), bf16),
            pltpu.VMEM((experts, cap, width), bf16),
            pltpu.VMEM((experts * 4, cap, width), bf16),
            pltpu.VMEM((4 * cap, hidden), bf16),
            pltpu.VMEM((experts * 4, cap, width), bf16),
            pltpu.VMEM((experts * 2, cap, width), bf16),
            pltpu.VMEM((experts * 2, cap, width), bf16),
            pltpu.VMEM((experts, cap, width), bf16),
            pltpu.VMEM((experts, cap, width), bf16),
            pltpu.VMEM((experts, cap, width), bf16),
            pltpu.VMEM((tiles, width, 2 * LANE), bf16),
            pltpu.VMEM((hidden, width), bf16),
            dma((tiles,)), dma((tiles,)), dma, dma,
        ] + [dma((PIECES * experts,))] * 8 + [dma((2 * PIECES * experts,))] * 2 + [dma((PIECES * experts,))] * 4,
        compiler_params=pltpu.CompilerParams(
            collective_id=0, has_side_effects=True, vmem_limit_bytes=60 * 1024 * 1024),
    )(tokens, norm_gain.reshape(1, -1), expert_ids.T, route_weights.T, w_gate, w_up, w_down)


def solution(mesh):
    placed = (
        P(("grp", "ep", "tp"), None),
        P(),
        P(("grp", "ep", "tp"), None),
        P(("grp", "ep", "tp"), None),
        P(None, ("ep", "tp")),
        P(None, ("ep", "tp")),
        P(("ep", "tp"), None),
    )
    return jax.shard_map(
        local, mesh=mesh, in_specs=placed, out_specs=P(("grp", "ep", "tp"), None), check_vma=False
    )
```

profile of v0, /device:TPU:8, one launch (start us, length us, event | category | flops | bytes accessed | tf_op | source)
XLA Modules:
  0.0 89.8 jit_solution(1932980102925092580)
XLA Ops:
  0.0 87.9 %shard_map.73 = bf16[128,2048]{1,0:T(8,128)(2,1)} custom-call(bf16[128,2048]{1,0:T(8,128)(2,1)} %tok_ref.1, f32[1,2048]{1,0:T(1,128)} %bitcast.3, s32[2,128]{1,0:T(2,128)} %bitcast.4, f32[2,128]{1,0:T(2,128)} %bitcast.5, bf16[2048,896]{1,0:T(8,128)(2,1)} %gate_ref.1, bf16[2048,896]{1,0:T(8,128)(2,1)} %up_ref.1, bf16[896,2048]{1,0:T(8,128)(2,1)} %down_ref.1), custom_call_target="tpu_custom_call" | custom-call | tf_op jit(solution)/shard_map/pallas_call | solution.py:331
  87.9 1.9 %copy.9 = bf16[128,2048]{1,0:T(8,128)(2,1)} copy(bf16[128,2048]{1,0:T(8,128)(2,1)} %shard_map.73) | data formatting | bytes 1048576
where the time goes:
time: 90.5 us; the launch traced here: 89.8 us
  Pallas kernels  87.9 us (97%)
  local copies, waits for them, and re-layouts  1.88 us (2%)
    pallas_call x1, Pallas kernels, local(): pl.pallas_call(functools.partial(kernel, experts, cap), out_shape=jax.Sha...  87.9 us
    unnamed x1, local copies, waits for them, and re-layouts  1.88 us

commit v1 on v0

--- a/solution.py
+++ b/solution.py
@@ -10,10 +10,15 @@
 MESH = pl.DeviceIdType.MESH
 LANE = 128
 PIECES = 2
-
-
-def turn(i, experts):
-    return i % experts
+STAGES = 0
+SCHEDULE = (
+    ("near", 0, 0, 0),
+    ("spread", -1, 1, 0),
+    ("pass_on", 0, 0, 0),
+    ("far", 0, 0, 0),
+    ("give", 0, 1, 0),
+    ("finish", 1, 1, -1),
+)
 
 
 def mix_index(first, second, count):
@@ -28,10 +33,10 @@
 
 def kernel(
     experts, cap,
-    tok_ref, gain_ref, ids_ref, weight_ref, gate_ref, up_ref, down_ref,
+    tok_hbm, gain_hbm, ids_hbm, weight_hbm, gate_ref, up_ref, down_ref,
     out_ref,
-    norm, xs, xa, hid, po, rd, cx, rx, fo, ret, wgu, wd,
-    gate_sem, up_sem, down_sem, own_sem,
+    tok_ref, gain_ref, ids_ref, weight_ref, norm, names, ranks, mixing, xs, xa, hid, po, rd, cx, rx, fo, ret, wgu, wd,
+    in_sem, gate_sem, up_sem, down_sem,
     z_send, z_recv, x_send, x_recv, d_send, d_recv, e_send, e_recv,
     r_send, r_recv, v_send, v_recv, w_send, w_recv,
 ):
@@ -46,6 +51,12 @@
     def plane(q):
         return {"ep": 2 * q + h, "tp": c}
 
+    loads = [
+        pltpu.make_async_copy(src, dst, in_sem.at[n]) for n, (src, dst) in enumerate((
+            (tok_hbm, tok_ref), (gain_hbm, gain_ref), (ids_hbm, ids_ref), (weight_hbm, weight_ref)))]
+    for load in loads:
+        load.start()
+
     barrier = pltpu.get_barrier_semaphore()
 
     def greet(k, carry):
@@ -70,14 +81,20 @@
         up_copy(j).start()
     down_copy.start()
 
-    values = tok_ref[...].astype(jnp.float32)
-    scale_rows = lax.rsqrt(jnp.mean(values * values, axis=1, keepdims=True) + 1e-06)
-    norm[...] = (values * scale_rows * gain_ref[...]).astype(jnp.bfloat16)
-
     row = lax.broadcasted_iota(jnp.int32, (toks, toks), 0)
     col = lax.broadcasted_iota(jnp.int32, (toks, toks), 1)
     before = (row < col).astype(jnp.float32).astype(jnp.bfloat16)
     slots = lax.broadcasted_iota(jnp.int32, (cap, toks), 0).astype(jnp.float32)
+    for load in loads[1:]:
+        load.wait()
+    kinds = lax.broadcasted_iota(jnp.int32, names.shape, 0)
+    names[...] = ((ids_ref[0:1, :] == kinds) | (ids_ref[1:2, :] == kinds)).astype(jnp.float32)
+    ranks[...] = jnp.dot(names[...].astype(jnp.bfloat16), before, preferred_element_type=jnp.float32)
+
+    loads[0].wait()
+    values = tok_ref[...].astype(jnp.float32)
+    scale_rows = lax.rsqrt(jnp.mean(values * values, axis=1, keepdims=True) + 1e-06)
+    norm[...] = (values * scale_rows * gain_ref[...]).astype(jnp.bfloat16)
 
     def remote(src, dst, send, recv, target):
         return pltpu.make_async_remote_copy(
@@ -98,8 +115,6 @@
     def z_land(k, g):
         return z_pair(k, g, lambda q: q)
 
-    own_copy = pltpu.make_async_copy(xs.at[p], xa.at[4 * p + 2 * h + c], own_sem)
-
     def mine(k, half, core, g):
         return cut(xa, 4 * mix_index(p, k, experts) + 2 * half + core, g)
 
@@ -146,61 +161,80 @@
     def w_land(k, g):
         return w_pair(k, g, lambda q: q)
 
+    def picked(e):
+        spot = pl.ds(e, 1)
+        pick = jnp.where(slots == ranks[spot, :], names[spot, :], 0.0).astype(jnp.bfloat16)
+        return jnp.dot(pick, norm[...], preferred_element_type=jnp.float32).astype(jnp.bfloat16)
+
     pl.semaphore_wait(barrier, experts + 1)
 
-    def fill(i, carry):
-        k = turn(i + 1, experts)
+    xa[4 * p + 2 * h + c] = picked(p)
+    for g in range(PIECES):
+        x_copy(0, g).start()
+        d_copy(0, g).start()
+
+    def fill(k, carry):
         e = mix_index(p, k, experts)
-        named = ((ids_ref[0:1, :] == e) | (ids_ref[1:2, :] == e)).astype(jnp.float32)
-        rank = jnp.dot(
-            jnp.broadcast_to(named, (16, toks)).astype(jnp.bfloat16), before,
-            preferred_element_type=jnp.float32)[0:1, :]
-        pick = jnp.where(slots == rank, named, 0.0).astype(jnp.bfloat16)
-        xs[e] = jnp.dot(pick, norm[...], preferred_element_type=jnp.float32).astype(jnp.bfloat16)
-
-        @pl.when(k > 0)
-        def _():
-            for g in range(PIECES):
-                z_copy(k, g).start()
-
+        xs[e] = picked(e)
+        for g in range(PIECES):
+            z_copy(k, g).start()
         return carry
 
-    lax.fori_loop(0, experts, fill, 0)
-    own_copy.start()
-    own_copy.wait()
+    lax.fori_loop(1, experts, fill, 0)
 
     step = 2 * LANE
 
-    def compute(k):
-        first = 4 * mix_index(p, k, experts)
-
-        def gate_up(j, carry):
-            rows = xa[pl.ds(first, 4)].reshape(4 * cap, width)
+    def compute(k, half):
+        rows = xa[pl.ds(4 * mix_index(p, k, experts) + 2 * half, 2)].reshape(2 * cap, width)
+        for j in range(tiles):
             both = jnp.dot(rows, wgu[j], preferred_element_type=jnp.float32)
             gate, up = both[:, :LANE], both[:, LANE:]
-            hid[:, pl.ds(pl.multiple_of(j * LANE, LANE), LANE)] = (
-                gate / (1.0 + jnp.exp(-gate)) * up).astype(jnp.bfloat16)
-            return carry
-
-        lax.fori_loop(0, tiles, gate_up, 0)
-
-        def down(n, carry):
-            place = pl.ds(pl.multiple_of(n * step, step), step)
-            part = jnp.dot(hid[...], wd[:, place], preferred_element_type=jnp.float32)
-            po[pl.ds(4 * k, 4), :, place] = part.astype(jnp.bfloat16).reshape(4, cap, step)
-            return carry
-
+            hid[:, j * LANE:(j + 1) * LANE] = (gate / (1.0 + jnp.exp(-gate)) * up).astype(jnp.bfloat16)
         many = part_width // step
         for g in range(PIECES):
-            lax.fori_loop(g * many, (g + 1) * many, down, 0)
-            for half in range(2):
-                r_copy(k, half, g).start()
+            for n in range(g * many, (g + 1) * many):
+                part = jnp.dot(hid[...], wd[:, n * step:(n + 1) * step], preferred_element_type=jnp.float32)
+                po[pl.ds(4 * k + 2 * half, 2), :, n * step:(n + 1) * step] = part.astype(
+                    jnp.bfloat16).reshape(2, cap, step)
+            r_copy(k, half, g).start()
 
     def add(first, second):
         return (first.astype(jnp.float32) + second.astype(jnp.float32)).astype(jnp.bfloat16)
 
+    def spread(k):
+        for g in range(PIECES):
+            z_land(k, g).wait_recv()
+            x_copy(k, g).start()
+            d_copy(k, g).start()
+
+    def pass_on(k):
+        for g in range(PIECES):
+            x_land(k, g).wait_recv()
+            e_copy(k, g).start()
+
+    def far(k):
+        for g in range(PIECES):
+            e_land(k, g).wait_recv()
+        compute(k, 1 - h)
+
+    def near(k):
+        for g in range(PIECES):
+            d_land(k, g).wait_recv()
+        compute(k, h)
+
+    def join(k, half, g):
+        cols = pl.ds(g * part_width, part_width)
+        r_copy(k, half, g).wait_recv()
+        cx[2 * k + half, :, cols] = add(po[4 * k + 2 * half + c, :, cols], rd[2 * k + half, :, cols])
+
+    def give(k):
+        for g in range(PIECES):
+            join(k, 1 - h, g)
+            v_copy(k, g).start()
+
     def finish(k):
         for g in range(PIECES):
+            join(k, h, g)
             v_copy(k, g).wait_recv()
             cols = pl.ds(g * part_width, part_width)
             total = add(cx[2 * k + h, :, cols], rx[k, :, cols])
@@ -215,56 +249,24 @@
                 w_copy(k, g).start()
 
     def stage(i, carry):
-        @pl.when(i < experts)
-        def _():
-            k = turn(i, experts)
-            for g in range(PIECES):
-                @pl.when(k > 0)
-                def _():
-                    z_land(k, g).wait_recv()
-
-                x_copy(k, g).start()
-                d_copy(k, g).start()
-
-        @pl.when(i > 0)
-        def _():
-            k = turn(i - 1, experts)
-            for g in range(PIECES):
-                x_land(k, g).wait_recv()
-                e_copy(k, g).start()
-
-            @pl.when(i == 1)
+        for event, lag, first, last in PLAN:
+            k = i - lag
+
+            @pl.when((k >= first) & (k < experts + last))
             def _():
-                for j in range(tiles):
-                    gate_copy(j).wait()
-                    up_copy(j).wait()
-                down_copy.wait()
-
-            for g in range(PIECES):
-                d_land(k, g).wait_recv()
-                e_land(k, g).wait_recv()
-            compute(k)
-
-            @pl.when(i > 2)
-            def _():
-                finish(turn(i - 2, experts))
-
-            for g in range(PIECES):
-                cols = pl.ds(g * part_width, part_width)
-                for half in range(2):
-                    r_copy(k, half, g).wait_recv()
-                    cx[2 * k + half, :, cols] = add(
-                        po[4 * k + 2 * half + c, :, cols], rd[2 * k + half, :, cols])
-
-                @pl.when(k > 0)
-                def _():
-                    v_copy(k, g).start()
+                event(k)
 
         return carry
 
-    lax.fori_loop(0, experts + 1, stage, 0)
-    for g in range(PIECES):
-        v_copy(0, g).start()
+    names_of = dict(spread=spread, pass_on=pass_on, far=far, near=near, give=give, finish=finish)
+    PLAN = [(names_of[n], lag, first, last) for n, lag, first, last in SCHEDULE]
+
+    for j in range(tiles):
+        gate_copy(j).wait()
+        up_copy(j).wait()
+    down_copy.wait()
+    lax.fori_loop(0, experts + STAGES, stage, 0)
+    give(0)
 
     def settle(k, carry):
         for g in range(PIECES):
@@ -300,7 +302,7 @@
     places = lax.fori_loop(0, experts, place_of, (zero, zero))
     lanes = lax.broadcasted_iota(jnp.int32, (toks, experts * cap), 1).astype(jnp.float32)
     picks = [(lanes == place).astype(jnp.float32).astype(jnp.bfloat16) for place in places]
-    finish(turn(experts - 1, experts))
+    finish(experts - 1)
     finish(0)
     lax.fori_loop(0, experts, settle, 0)
     for g in range(PIECES):
@@ -325,19 +327,27 @@
     capacity = 2 * max(1, 5 * toks * expert_ids.shape[1] // (8 * experts))
     cap = -(-capacity // 16) * 16
     tiles = hidden // LANE
-    vmem, any_space = pl.BlockSpec(memory_space=pltpu.VMEM), pl.BlockSpec(memory_space=pl.ANY)
+    kinds = -(-experts // 16) * 16
+    any_space = pl.BlockSpec(memory_space=pl.ANY)
     dma = pltpu.SemaphoreType.DMA
     bf16 = jnp.bfloat16
     return pl.pallas_call(
         functools.partial(kernel, experts, cap),
-        out_shape=jax.ShapeDtypeStruct((toks, width), bf16),
-        in_specs=[vmem] * 4 + [any_space] * 3,
-        out_specs=vmem,
+        out_shape=pltpu.VMEM((toks, width), bf16),
+        in_specs=[any_space] * 7,
+        out_specs=pl.BlockSpec(memory_space=pltpu.VMEM),
         scratch_shapes=[
             pltpu.VMEM((toks, width), bf16),
+            pltpu.VMEM((1, width), jnp.float32),
+            pltpu.VMEM((2, toks), jnp.int32),
+            pltpu.VMEM((2, toks), jnp.float32),
+            pltpu.VMEM((toks, width), bf16),
+            pltpu.VMEM((kinds, toks), jnp.float32),
+            pltpu.VMEM((kinds, toks), jnp.float32),
+            pltpu.VMEM((8, LANE), jnp.float32),
             pltpu.VMEM((experts, cap, width), bf16),
             pltpu.VMEM((experts * 4, cap, width), bf16),
-            pltpu.VMEM((4 * cap, hidden), bf16),
+            pltpu.VMEM((2 * cap, hidden), bf16),
             pltpu.VMEM((experts * 4, cap, width), bf16),
             pltpu.VMEM((experts * 2, cap, width), bf16),
             pltpu.VMEM((experts * 2, cap, width), bf16),
@@ -346,7 +356,7 @@
             pltpu.VMEM((experts, cap, width), bf16),
             pltpu.VMEM((tiles, width, 2 * LANE), bf16),
             pltpu.VMEM((hidden, width), bf16),
-            dma((tiles,)), dma((tiles,)), dma, dma,
+            dma((4,)), dma((tiles,)), dma((tiles,)), dma,
         ] + [dma((PIECES * experts,))] * 8 + [dma((2 * PIECES * experts,))] * 2 + [dma((PIECES * experts,))] * 4,
         compiler_params=pltpu.CompilerParams(
             collective_id=0, has_side_effects=True, vmem_limit_bytes=60 * 1024 * 1024),

time: 90.5 us -> 79.7 us (0.88)
  Pallas kernels: 87.9 us -> 78.5 us
  local copies, waits for them, and re-layouts: 1.88 us -> 0.8 us
    pallas_call x1, Pallas kernels: 87.9 us -> 78.5 us  [local(): pl.pallas_call(functools.partial(kernel, experts, cap), out_shape=pltpu.V...]
    unnamed x1, local copies, waits for them, and re-layouts: 1.88 us -> 0.8 us
where the time goes in v1:
time: 79.7 us; the launch traced here: 79.3 us
  Pallas kernels  78.5 us (98%)
  local copies, waits for them, and re-layouts  0.8 us (1%)
    pallas_call x1, Pallas kernels, local(): pl.pallas_call(functools.partial(kernel, experts, cap), out_shape=pltpu.V...  78.5 us

profile of v1, /device:TPU:8, one launch (start us, length us, event | category | flops | bytes accessed | tf_op | source)
XLA Modules:
  0.0 79.3 jit_solution(10614904600993546206)
XLA Ops:
  0.0 78.5 %shard_map.73 = bf16[128,2048]{1,0:T(8,128)(2,1)S(1)} custom-call(bf16[128,2048]{1,0:T(8,128)(2,1)} %tok_hbm.1, f32[1,2048]{1,0:T(1,128)} %bitcast.3, s32[2,128]{1,0:T(2,128)} %bitcast.4, f32[2,128]{1,0:T(2,128)} %bitcast.5, bf16[2048,896]{1,0:T(8,128)(2,1)} %gate_ref.1, bf16[2048,896]{1,0:T(8,128)(2,1)} %up_ref.1, bf16[896,2048]{1,0:T(8,128)(2,1)} %down_ref.1), custom_call_target="tpu_custom_call" | custom-call | tf_op jit(solution)/shard_map/pallas_call | solution.py:334
  78.5 0.8 %copy.9 = bf16[128,2048]{1,0:T(8,128)(2,1)} copy(bf16[128,2048]{1,0:T(8,128)(2,1)S(1)} %shard_map.73) | data formatting | bytes 1048576

commit v2 on v1

--- a/solution.py
+++ b/solution.py
@@ -10,14 +10,50 @@
 MESH = pl.DeviceIdType.MESH
 LANE = 128
 PIECES = 2
-STAGES = 0
-SCHEDULE = (
-    ("near", 0, 0, 0),
-    ("spread", -1, 1, 0),
-    ("pass_on", 0, 0, 0),
-    ("far", 0, 0, 0),
-    ("give", 0, 1, 0),
-    ("finish", 1, 1, -1),
+TURNS = ((0, 2, 3, 1), (0, 3, 2, 1))
+SENDS = (
+    ((2, 1), (2, 0), (1, 1), (1, 0), (3, 1), (3, 0)),
+    ((3, 1), (2, 0), (2, 1), (3, 0), (1, 0), (1, 1)),
+)
+ORDER = (
+    ("spread", 2, 1),
+    ("spread", 2, 0),
+    ("spread", 3, 1),
+    ("near", 2),
+    ("spread", 3, 0),
+    ("pass_on", 2, 0),
+    ("pass_on", 2, 1),
+    ("spread", 1, 0),
+    ("far", 2),
+    ("spread", 1, 1),
+    ("give", 2, 0),
+    ("pass_on", 3, 1),
+    ("pass_on", 3, 0),
+    ("near", 3),
+    ("pass_on", 0, 1),
+    ("far", 3),
+    ("give", 2, 1),
+    ("pass_on", 1, 1),
+    ("give", 3, 1),
+    ("pass_on", 1, 0),
+    ("finish", 2, 0),
+    ("pass_on", 0, 0),
+    ("far", 1),
+    ("finish", 2, 1),
+    ("give", 3, 0),
+    ("far", 0),
+    ("finish", 3, 1),
+    ("give", 1, 1),
+    ("give", 1, 0),
+    ("near", 1),
+    ("give", 0, 1),
+    ("finish", 3, 0),
+    ("finish", 1, 1),
+    ("give", 0, 0),
+    ("near", 0),
+    ("finish", 1, 0),
+    ("finish", 0, 1),
+    ("finish", 0, 0),
 )
 
 
@@ -35,7 +71,7 @@
     experts, cap,
     tok_hbm, gain_hbm, ids_hbm, weight_hbm, gate_ref, up_ref, down_ref,
     out_ref,
-    tok_ref, gain_ref, ids_ref, weight_ref, norm, names, ranks, mixing, xs, xa, hid, po, rd, cx, rx, fo, ret, wgu, wd,
+    tok_ref, gain_ref, ids_ref, weight_ref, norm, names, ranks, sides, picks, xs, xa, hid, po, rd, cx, rx, fo, ret, wgu, wd,
     in_sem, gate_sem, up_sem, down_sem,
     z_send, z_recv, x_send, x_recv, d_send, d_recv, e_send, e_recv,
     r_send, r_recv, v_send, v_recv, w_send, w_recv,
@@ -148,7 +184,7 @@
 
     def v_copy(k, g):
         n = PIECES * k + g
-        return remote(cut(cx, 2 * k + 1 - h, g), cut(rx, k, g), v_send.at[n], v_recv.at[n], across)
+        return remote(cut(cx, k, g), cut(rx, k, g), v_send.at[n], v_recv.at[n], across)
 
     def w_pair(k, g, origin):
         q = mix_index(p, k, experts)
@@ -166,6 +202,12 @@
         pick = jnp.where(slots == ranks[spot, :], names[spot, :], 0.0).astype(jnp.bfloat16)
         return jnp.dot(pick, norm[...], preferred_element_type=jnp.float32).astype(jnp.bfloat16)
 
+    inner = (p + 1) // 2 % 2
+
+    def turn(s):
+        outside, inside = TURNS[0][s], TURNS[1][s]
+        return outside if outside == inside else outside + inner * (inside - outside)
+
     pl.semaphore_wait(barrier, experts + 1)
 
     xa[4 * p + 2 * h + c] = picked(p)
@@ -173,14 +215,23 @@
         x_copy(0, g).start()
         d_copy(0, g).start()
 
-    def fill(k, carry):
-        e = mix_index(p, k, experts)
-        xs[e] = picked(e)
-        for g in range(PIECES):
-            z_copy(k, g).start()
-        return carry
-
-    lax.fori_loop(1, experts, fill, 0)
+    if experts == len(TURNS[0]):
+        for k in range(1, experts):
+            xs[mix_index(p, k, experts)] = picked(mix_index(p, k, experts))
+        for side, sends in enumerate(SENDS):
+            @pl.when(inner == side)
+            def _():
+                for s, g in sends:
+                    z_copy(TURNS[side][s], g).start()
+    else:
+        def fill(k, carry):
+            e = mix_index(p, k, experts)
+            xs[e] = picked(e)
+            for g in range(PIECES):
+                z_copy(k, g).start()
+            return carry
+
+        lax.fori_loop(1, experts, fill, 0)
 
     step = 2 * LANE
 
@@ -201,16 +252,14 @@
     def add(first, second):
         return (first.astype(jnp.float32) + second.astype(jnp.float32)).astype(jnp.bfloat16)
 
-    def spread(k):
-        for g in range(PIECES):
-            z_land(k, g).wait_recv()
-            x_copy(k, g).start()
-            d_copy(k, g).start()
-
-    def pass_on(k):
-        for g in range(PIECES):
-            x_land(k, g).wait_recv()
-            e_copy(k, g).start()
+    def spread(k, g):
+        z_land(k, g).wait_recv()
+        x_copy(k, g).start()
+        d_copy(k, g).start()
+
+    def pass_on(k, g):
+        x_land(k, g).wait_recv()
+        e_copy(k, g).start()
 
     def far(k):
         for g in range(PIECES):
@@ -222,51 +271,84 @@
             d_land(k, g).wait_recv()
         compute(k, h)
 
-    def join(k, half, g):
+    def joined(k, half, g):
         cols = pl.ds(g * part_width, part_width)
         r_copy(k, half, g).wait_recv()
-        cx[2 * k + half, :, cols] = add(po[4 * k + 2 * half + c, :, cols], rd[2 * k + half, :, cols])
-
-    def give(k):
-        for g in range(PIECES):
-            join(k, 1 - h, g)
-            v_copy(k, g).start()
-
-    def finish(k):
-        for g in range(PIECES):
-            join(k, h, g)
-            v_copy(k, g).wait_recv()
-            cols = pl.ds(g * part_width, part_width)
-            total = add(cx[2 * k + h, :, cols], rx[k, :, cols])
-
-            @pl.when(k == 0)
-            def _():
-                ret[p, :, cols] = total
-
-            @pl.when(k > 0)
-            def _():
-                fo[k, :, cols] = total
-                w_copy(k, g).start()
-
-    def stage(i, carry):
-        for event, lag, first, last in PLAN:
-            k = i - lag
-
-            @pl.when((k >= first) & (k < experts + last))
-            def _():
-                event(k)
-
-        return carry
-
-    names_of = dict(spread=spread, pass_on=pass_on, far=far, near=near, give=give, finish=finish)
-    PLAN = [(names_of[n], lag, first, last) for n, lag, first, last in SCHEDULE]
+        return add(po[4 * k + 2 * half + c, :, cols], rd[2 * k + half, :, cols])
+
+    def give(k, g):
+        cx[k, :, g * part_width:(g + 1) * part_width] = joined(k, 1 - h, g)
+        v_copy(k, g).start()
+
+    def finish(k, g):
+        cols = pl.ds(g * part_width, part_width)
+        here = joined(k, h, g)
+        v_copy(k, g).wait_recv()
+        total = add(here, rx[k, :, cols])
+        if isinstance(k, int) and k == 0:
+            ret[p, :, cols] = total
+        else:
+            fo[k, :, cols] = total
+            w_copy(k, g).start()
+
+    after = (col < row).astype(jnp.float32).astype(jnp.bfloat16)
+
+    sides[...] = jnp.concatenate(
+        [ids_ref[...].astype(jnp.float32), weight_ref[...], jnp.zeros((LANE - 4, toks), jnp.float32)], axis=0).T
+
+    def place_of(e, places):
+        number = lax.convert_element_type(e, jnp.float32)
+        hits = [(sides[:, n:n + 1] == number).astype(jnp.float32) for n in range(2)]
+        rank = jnp.dot(
+            after, jnp.broadcast_to(hits[0] + hits[1], (toks, LANE)).astype(jnp.bfloat16),
+            preferred_element_type=jnp.float32)[:, 0:1]
+        spot = rank + number * cap
+        return tuple(old + hit * spot for old, hit in zip(places, hits))
+
+    zero = jnp.zeros((toks, 1), jnp.float32)
+    places = lax.fori_loop(0, experts, place_of, (zero, zero))
+    lanes = lax.broadcasted_iota(jnp.int32, (toks, experts * cap), 1).astype(jnp.float32)
+    for m in range(2):
+        picks[m] = (lanes == places[m]).astype(jnp.float32).astype(jnp.bfloat16)
 
     for j in range(tiles):
         gate_copy(j).wait()
         up_copy(j).wait()
     down_copy.wait()
-    lax.fori_loop(0, experts + STAGES, stage, 0)
-    give(0)
+
+    events = dict(spread=spread, pass_on=pass_on, far=far, near=near, give=give, finish=finish)
+    if experts == len(TURNS[0]):
+        for name, s, *g in ORDER:
+            events[name](turn(s), *g)
+    else:
+        def each(event, k):
+            for g in range(PIECES):
+                event(k, g)
+
+        def stage(k, carry):
+            near(k)
+
+            @pl.when(k + 1 < experts)
+            def _():
+                each(spread, k + 1)
+
+            each(pass_on, k)
+            far(k)
+
+            @pl.when(k > 1)
+            def _():
+                each(finish, k - 1)
+
+            @pl.when(k > 0)
+            def _():
+                each(give, k)
+
+            return carry
+
+        lax.fori_loop(0, experts, stage, 0)
+        each(give, 0)
+        each(finish, experts - 1)
+        each(finish, 0)
 
     def settle(k, carry):
         for g in range(PIECES):
@@ -284,27 +366,6 @@
 
         return carry
 
-    after = (col < row).astype(jnp.float32).astype(jnp.bfloat16)
-
-    sides = jnp.concatenate(
-        [ids_ref[...].astype(jnp.float32), weight_ref[...], jnp.zeros((LANE - 4, toks), jnp.float32)], axis=0).T
-
-    def place_of(e, places):
-        number = lax.convert_element_type(e, jnp.float32)
-        hits = [(sides[:, n:n + 1] == number).astype(jnp.float32) for n in range(2)]
-        rank = jnp.dot(
-            after, jnp.broadcast_to(hits[0] + hits[1], (toks, LANE)).astype(jnp.bfloat16),
-            preferred_element_type=jnp.float32)[:, 0:1]
-        spot = rank + number * cap
-        return tuple(old + hit * spot for old, hit in zip(places, hits))
-
-    zero = jnp.zeros((toks, 1), jnp.float32)
-    places = lax.fori_loop(0, experts, place_of, (zero, zero))
-    lanes = lax.broadcasted_iota(jnp.int32, (toks, experts * cap), 1).astype(jnp.float32)
-    picks = [(lanes == place).astype(jnp.float32).astype(jnp.bfloat16) for place in places]
-    finish(experts - 1)
-    finish(0)
-    lax.fori_loop(0, experts, settle, 0)
     for g in range(PIECES):
         def landed(k, carry):
             w_land(k, g).wait_recv()
@@ -318,6 +379,7 @@
             total = total + sides[:, 2 + m:3 + m] * jnp.dot(
                 picks[m], rows, preferred_element_type=jnp.float32)
         out_ref[:, cols] = total.astype(jnp.bfloat16)
+    lax.fori_loop(0, experts, settle, 0)
 
 
 def local(tokens, norm_gain, expert_ids, route_weights, w_gate, w_up, w_down):
@@ -344,13 +406,14 @@
             pltpu.VMEM((toks, width), bf16),
             pltpu.VMEM((kinds, toks), jnp.float32),
             pltpu.VMEM((kinds, toks), jnp.float32),
-            pltpu.VMEM((8, LANE), jnp.float32),
+            pltpu.VMEM((toks, LANE), jnp.float32),
+            pltpu.VMEM((2, toks, experts * cap), bf16),
             pltpu.VMEM((experts, cap, width), bf16),
             pltpu.VMEM((experts * 4, cap, width), bf16),
             pltpu.VMEM((2 * cap, hidden), bf16),
             pltpu.VMEM((experts * 4, cap, width), bf16),
             pltpu.VMEM((experts * 2, cap, width), bf16),
-            pltpu.VMEM((experts * 2, cap, width), bf16),
+            pltpu.VMEM((experts, cap, width), bf16),
             pltpu.VMEM((experts, cap, width), bf16),
             pltpu.VMEM((experts, cap, width), bf16),
             pltpu.VMEM((experts, cap, width), bf16),

time: 79.7 us -> 71 us (0.89)
  Pallas kernels: 78.5 us -> 70 us
    pallas_call x1, Pallas kernels: 78.5 us -> 70 us  [local(): pl.pallas_call(functools.partial(kernel, experts, cap), out_shape=pltpu.V...]
where the time goes in v2:
time: 71 us; the launch traced here: 70.8 us
  Pallas kernels  70 us (99%)
  local copies, waits for them, and re-layouts  0.8 us (1%)
    pallas_call x1, Pallas kernels, local(): pl.pallas_call(functools.partial(kernel, experts, cap), out_shape=pltpu.V...  70 us

profile of v2, /device:TPU:8, one launch (start us, length us, event | category | flops | bytes accessed | tf_op | source)
XLA Modules:
  0.0 70.8 jit_solution(4488923219018307729)
XLA Ops:
  0.0 70.0 %shard_map.73 = bf16[128,2048]{1,0:T(8,128)(2,1)S(1)} custom-call(bf16[128,2048]{1,0:T(8,128)(2,1)} %tok_hbm.1, f32[1,2048]{1,0:T(1,128)} %bitcast.3, s32[2,128]{1,0:T(2,128)} %bitcast.4, f32[2,128]{1,0:T(2,128)} %bitcast.5, bf16[2048,896]{1,0:T(8,128)(2,1)} %gate_ref.1, bf16[2048,896]{1,0:T(8,128)(2,1)} %up_ref.1, bf16[896,2048]{1,0:T(8,128)(2,1)} %down_ref.1), custom_call_target="tpu_custom_call" | custom-call | tf_op jit(solution)/shard_map/pallas_call | solution.py:396
  70.0 0.8 %copy.9 = bf16[128,2048]{1,0:T(8,128)(2,1)} copy(bf16[128,2048]{1,0:T(8,128)(2,1)S(1)} %shard_map.73) | data formatting | bytes 1048576

commit v3 on v2

--- a/solution.py
+++ b/solution.py
@@ -10,50 +10,50 @@
 MESH = pl.DeviceIdType.MESH
 LANE = 128
 PIECES = 2
-TURNS = ((0, 2, 3, 1), (0, 3, 2, 1))
+TURNS = ((0, 2, 1, 3), (0, 3, 1, 2))
 SENDS = (
-    ((2, 1), (2, 0), (1, 1), (1, 0), (3, 1), (3, 0)),
-    ((3, 1), (2, 0), (2, 1), (3, 0), (1, 0), (1, 1)),
+    ((3, 0), (3, 1), (1, 0), (1, 1), (2, 1), (2, 0)),
+    ((3, 1), (2, 1), (1, 1), (2, 0), (3, 0), (1, 0)),
 )
 ORDER = (
+    ("spread", 3, 0),
+    ("spread", 3, 1),
     ("spread", 2, 1),
+    ("pass_on", 0, 0),
+    ("pass_on", 3, 0),
+    ("pass_on", 0, 1),
+    ("pass_on", 3, 1),
     ("spread", 2, 0),
-    ("spread", 3, 1),
+    ("far", 3),
+    ("pass_on", 2, 1),
+    ("spread", 1, 1),
     ("near", 2),
-    ("spread", 3, 0),
+    ("give", 3, 1),
     ("pass_on", 2, 0),
-    ("pass_on", 2, 1),
+    ("near", 3),
     ("spread", 1, 0),
+    ("give", 3, 0),
+    ("pass_on", 1, 1),
     ("far", 2),
-    ("spread", 1, 1),
+    ("near", 1),
+    ("finish", 3, 1),
     ("give", 2, 0),
-    ("pass_on", 3, 1),
-    ("pass_on", 3, 0),
-    ("near", 3),
-    ("pass_on", 0, 1),
-    ("far", 3),
+    ("pass_on", 1, 0),
+    ("far", 0),
+    ("finish", 3, 0),
     ("give", 2, 1),
-    ("pass_on", 1, 1),
-    ("give", 3, 1),
-    ("pass_on", 1, 0),
+    ("far", 1),
     ("finish", 2, 0),
-    ("pass_on", 0, 0),
-    ("far", 1),
+    ("give", 1, 0),
+    ("give", 1, 1),
+    ("near", 0),
     ("finish", 2, 1),
-    ("give", 3, 0),
-    ("far", 0),
-    ("finish", 3, 1),
-    ("give", 1, 1),
-    ("give", 1, 0),
-    ("near", 1),
+    ("finish", 1, 0),
+    ("give", 0, 0),
     ("give", 0, 1),
-    ("finish", 3, 0),
     ("finish", 1, 1),
-    ("give", 0, 0),
-    ("near", 0),
-    ("finish", 1, 0),
+    ("finish", 0, 0),
     ("finish", 0, 1),
-    ("finish", 0, 0),
 )
 
 
@@ -72,7 +72,7 @@
     tok_hbm, gain_hbm, ids_hbm, weight_hbm, gate_ref, up_ref, down_ref,
     out_ref,
     tok_ref, gain_ref, ids_ref, weight_ref, norm, names, ranks, sides, picks, xs, xa, hid, po, rd, cx, rx, fo, ret, wgu, wd,
-    in_sem, gate_sem, up_sem, down_sem,
+    in_sem, wgu_sem, wd_sem,
     z_send, z_recv, x_send, x_recv, d_send, d_recv, e_send, e_recv,
     r_send, r_recv, v_send, v_recv, w_send, w_recv,
 ):
@@ -105,13 +105,13 @@
 
     def gate_copy(j):
         return pltpu.make_async_copy(
-            gate_ref.at[:, pl.ds(j * LANE, LANE)], wgu.at[j, :, pl.ds(0, LANE)], gate_sem.at[j])
+            gate_ref.at[:, pl.ds(j * LANE, LANE)], wgu.at[j, :, pl.ds(0, LANE)], wgu_sem)
 
     def up_copy(j):
         return pltpu.make_async_copy(
-            up_ref.at[:, pl.ds(j * LANE, LANE)], wgu.at[j, :, pl.ds(LANE, LANE)], up_sem.at[j])
-
-    down_copy = pltpu.make_async_copy(down_ref, wd, down_sem)
+            up_ref.at[:, pl.ds(j * LANE, LANE)], wgu.at[j, :, pl.ds(LANE, LANE)], wgu_sem)
+
+    down_copy = pltpu.make_async_copy(down_ref, wd, wd_sem)
     for j in range(tiles):
         gate_copy(j).start()
         up_copy(j).start()
@@ -141,9 +141,9 @@
 
     def z_pair(k, g, origin):
         q = mix_index(p, k, experts)
-        n = PIECES * k + g
+        n = PIECES * (k - 1) + g
         return remote(
-            cut(xs, q, g), cut(xa, 4 * origin(q) + 2 * h + c, g), z_send.at[n], z_recv.at[n], plane(q))
+            cut(xs, q, g), cut(xa, 4 * origin(q) + 2 * h + c, g), z_send, z_recv.at[n], plane(q))
 
     def z_copy(k, g):
         return z_pair(k, g, lambda q: p)
@@ -154,48 +154,41 @@
     def mine(k, half, core, g):
         return cut(xa, 4 * mix_index(p, k, experts) + 2 * half + core, g)
 
-    def shift(k, g, there, here, send, recv, target):
-        n = PIECES * k + g
-        return remote(mine(k, *there, g), mine(k, *here, g), send.at[n], recv.at[n], target)
-
     def x_copy(k, g):
-        return shift(k, g, (h, c), (h, c), x_send, x_recv, across)
+        return remote(mine(k, h, c, g), mine(k, h, c, g), x_send, x_recv.at[PIECES * k + g], across)
 
     def x_land(k, g):
-        return shift(k, g, (h, c), (1 - h, c), x_send, x_recv, across)
+        return remote(mine(k, h, c, g), mine(k, 1 - h, c, g), x_send, x_recv.at[PIECES * k + g], across)
 
     def d_copy(k, g):
-        return shift(k, g, (h, c), (h, c), d_send, d_recv, beside)
-
-    def d_land(k, g):
-        return shift(k, g, (h, c), (h, 1 - c), d_send, d_recv, beside)
+        return remote(mine(k, h, c, g), mine(k, h, c, g), d_send, d_recv.at[k], beside)
 
     def e_copy(k, g):
-        return shift(k, g, (1 - h, c), (1 - h, c), e_send, e_recv, beside)
-
-    def e_land(k, g):
-        return shift(k, g, (1 - h, c), (1 - h, 1 - c), e_send, e_recv, beside)
+        return remote(mine(k, 1 - h, c, g), mine(k, 1 - h, c, g), e_send, e_recv.at[k], beside)
+
+    def landing(k, half, send, recv):
+        first = 4 * mix_index(p, k, experts) + 2 * half
+        return remote(xa.at[first + c], xa.at[first + 1 - c], send, recv.at[k], beside)
 
     def r_copy(k, half, g):
         n = 2 * (PIECES * k + g) + half
         return remote(
             cut(po, 4 * k + 2 * half + 1 - c, g), cut(rd, 2 * k + half, g),
-            r_send.at[n], r_recv.at[n], beside)
+            r_send, r_recv.at[n], beside)
 
     def v_copy(k, g):
         n = PIECES * k + g
-        return remote(cut(cx, k, g), cut(rx, k, g), v_send.at[n], v_recv.at[n], across)
-
-    def w_pair(k, g, origin):
+        return remote(cut(cx, k, g), cut(rx, k, g), v_send, v_recv.at[n], across)
+
+    def w_copy(k, g):
         q = mix_index(p, k, experts)
-        n = PIECES * k + g
-        return remote(cut(fo, k, g), cut(ret, origin(q), g), w_send.at[n], w_recv.at[n], plane(q))
-
-    def w_copy(k, g):
-        return w_pair(k, g, lambda q: p)
-
-    def w_land(k, g):
-        return w_pair(k, g, lambda q: q)
+        return remote(cut(fo, k, g), cut(ret, p, g), w_send, w_recv.at[g], plane(q))
+
+    def w_land(g):
+        cols = pl.ds(g * part_width, part_width)
+        return remote(
+            fo.at[pl.ds(0, experts - 1), :, cols], ret.at[pl.ds(0, experts - 1), :, cols],
+            w_send, w_recv.at[g], beside)
 
     def picked(e):
         spot = pl.ds(e, 1)
@@ -262,13 +255,11 @@
         e_copy(k, g).start()
 
     def far(k):
-        for g in range(PIECES):
-            e_land(k, g).wait_recv()
+        landing(k, 1 - h, e_send, e_recv).wait_recv()
         compute(k, 1 - h)
 
     def near(k):
-        for g in range(PIECES):
-            d_land(k, g).wait_recv()
+        landing(k, h, d_send, d_recv).wait_recv()
         compute(k, h)
 
     def joined(k, half, g):
@@ -311,14 +302,26 @@
     for m in range(2):
         picks[m] = (lanes == places[m]).astype(jnp.float32).astype(jnp.bfloat16)
 
-    for j in range(tiles):
-        gate_copy(j).wait()
-        up_copy(j).wait()
+    pltpu.make_async_copy(wgu, wgu, wgu_sem).wait()
     down_copy.wait()
+
+    def sent(ref, count, send, recv):
+        part = ref.at[pl.ds(0, count)]
+        remote(part, part, send, recv.at[0], beside).wait_send()
+
+    def settle():
+        sent(xs, experts - 1, z_send, z_recv)
+        sent(xa, experts, x_send, x_recv)
+        sent(xa, experts, d_send, d_recv)
+        sent(xa, experts, e_send, e_recv)
+        sent(po, 2 * experts, r_send, r_recv)
 
     events = dict(spread=spread, pass_on=pass_on, far=far, near=near, give=give, finish=finish)
     if experts == len(TURNS[0]):
-        for name, s, *g in ORDER:
+        for name, s, *g in ORDER[:-1]:
+            events[name](turn(s), *g)
+        settle()
+        for name, s, *g in ORDER[-1:]:
             events[name](turn(s), *g)
     else:
         def each(event, k):
@@ -348,30 +351,11 @@
         lax.fori_loop(0, experts, stage, 0)
         each(give, 0)
         each(finish, experts - 1)
+        settle()
         each(finish, 0)
 
-    def settle(k, carry):
-        for g in range(PIECES):
-            x_copy(k, g).wait_send()
-            d_copy(k, g).wait_send()
-            e_copy(k, g).wait_send()
-            r_copy(k, 0, g).wait_send()
-            r_copy(k, 1, g).wait_send()
-            v_copy(k, g).wait_send()
-
-            @pl.when(k > 0)
-            def _():
-                z_copy(k, g).wait_send()
-                w_copy(k, g).wait_send()
-
-        return carry
-
     for g in range(PIECES):
-        def landed(k, carry):
-            w_land(k, g).wait_recv()
-            return carry
-
-        lax.fori_loop(1, experts, landed, 0)
+        w_land(g).wait_recv()
         cols = pl.ds(g * part_width, part_width)
         rows = ret[:, :, cols].reshape(experts * cap, part_width)
         total = jnp.zeros((toks, part_width), jnp.float32)
@@ -379,7 +363,8 @@
             total = total + sides[:, 2 + m:3 + m] * jnp.dot(
                 picks[m], rows, preferred_element_type=jnp.float32)
         out_ref[:, cols] = total.astype(jnp.bfloat16)
-    lax.fori_loop(0, experts, settle, 0)
+    sent(cx, experts, v_send, v_recv)
+    sent(fo, experts - 1, w_send, w_recv)
 
 
 def local(tokens, norm_gain, expert_ids, route_weights, w_gate, w_up, w_down):
@@ -419,8 +404,11 @@
             pltpu.VMEM((experts, cap, width), bf16),
             pltpu.VMEM((tiles, width, 2 * LANE), bf16),
             pltpu.VMEM((hidden, width), bf16),
-            dma((4,)), dma((tiles,)), dma((tiles,)), dma,
-        ] + [dma((PIECES * experts,))] * 8 + [dma((2 * PIECES * experts,))] * 2 + [dma((PIECES * experts,))] * 4,
+            dma((4,)), dma, dma,
+            dma, dma((PIECES * (experts - 1),)), dma, dma((PIECES * experts,)),
+            dma, dma((experts,)), dma, dma((experts,)),
+            dma, dma((2 * PIECES * experts,)), dma, dma((PIECES * experts,)), dma, dma((PIECES,)),
+        ],
         compiler_params=pltpu.CompilerParams(
             collective_id=0, has_side_effects=True, vmem_limit_bytes=60 * 1024 * 1024),
     )(tokens, norm_gain.reshape(1, -1), expert_ids.T, route_weights.T, w_gate, w_up, w_down)

time: 71 us -> 69.7 us (0.982)
  Pallas kernels: 70 us -> 68.7 us
    pallas_call x1, Pallas kernels: 70 us -> 68.7 us  [local(): pl.pallas_call(functools.partial(kernel, experts, cap), out_shape=pltpu.V...]
where the time goes in v3:
time: 69.7 us; the launch traced here: 69.5 us
  Pallas kernels  68.7 us (99%)
  local copies, waits for them, and re-layouts  0.8 us (1%)
    pallas_call x1, Pallas kernels, local(): pl.pallas_call(functools.partial(kernel, experts, cap), out_shape=pltpu.V...  68.7 us

profile of v3, /device:TPU:8, one launch (start us, length us, event | category | flops | bytes accessed | tf_op | source)
XLA Modules:
  0.0 69.5 jit_solution(12871320912580317943)
XLA Ops:
  0.0 68.7 %shard_map.73 = bf16[128,2048]{1,0:T(8,128)(2,1)S(1)} custom-call(bf16[128,2048]{1,0:T(8,128)(2,1)} %tok_hbm.1, f32[1,2048]{1,0:T(1,128)} %bitcast.3, s32[2,128]{1,0:T(2,128)} %bitcast.4, f32[2,128]{1,0:T(2,128)} %bitcast.5, bf16[2048,896]{1,0:T(8,128)(2,1)} %gate_ref.1, bf16[2048,896]{1,0:T(8,128)(2,1)} %up_ref.1, bf16[896,2048]{1,0:T(8,128)(2,1)} %down_ref.1), custom_call_target="tpu_custom_call" | custom-call | tf_op jit(solution)/shard_map/pallas_call | solution.py:381
  68.7 0.8 %copy.9 = bf16[128,2048]{1,0:T(8,128)(2,1)} copy(bf16[128,2048]{1,0:T(8,128)(2,1)S(1)} %shard_map.73) | data formatting | bytes 1048576

commit v4 on v3

--- a/solution.py
+++ b/solution.py
@@ -9,51 +9,179 @@
 
 MESH = pl.DeviceIdType.MESH
 LANE = 128
-PIECES = 2
-TURNS = ((0, 2, 1, 3), (0, 3, 1, 2))
+PIECES = 4
+TURNS = ((0, 1, 3, 2), (0, 3, 2, 1))
 SENDS = (
-    ((3, 0), (3, 1), (1, 0), (1, 1), (2, 1), (2, 0)),
-    ((3, 1), (2, 1), (1, 1), (2, 0), (3, 0), (1, 0)),
+    (
+        (2, 3),
+        (1, 1),
+        (3, 1),
+        (1, 0),
+        (3, 2),
+        (3, 3),
+        (3, 0),
+        (2, 2),
+        (2, 0),
+        (2, 1),
+        (1, 3),
+        (1, 2),
+    ),
+    (
+        (2, 2),
+        (3, 1),
+        (1, 1),
+        (3, 3),
+        (1, 3),
+        (2, 0),
+        (3, 2),
+        (2, 1),
+        (2, 3),
+        (3, 0),
+        (1, 0),
+        (1, 2),
+    ),
 )
-ORDER = (
-    ("spread", 3, 0),
-    ("spread", 3, 1),
-    ("spread", 2, 1),
-    ("pass_on", 0, 0),
-    ("pass_on", 3, 0),
-    ("pass_on", 0, 1),
-    ("pass_on", 3, 1),
-    ("spread", 2, 0),
-    ("far", 3),
-    ("pass_on", 2, 1),
-    ("spread", 1, 1),
-    ("near", 2),
-    ("give", 3, 1),
-    ("pass_on", 2, 0),
-    ("near", 3),
-    ("spread", 1, 0),
-    ("give", 3, 0),
-    ("pass_on", 1, 1),
-    ("far", 2),
-    ("near", 1),
-    ("finish", 3, 1),
-    ("give", 2, 0),
-    ("pass_on", 1, 0),
-    ("far", 0),
-    ("finish", 3, 0),
-    ("give", 2, 1),
-    ("far", 1),
-    ("finish", 2, 0),
-    ("give", 1, 0),
-    ("give", 1, 1),
-    ("near", 0),
-    ("finish", 2, 1),
-    ("finish", 1, 0),
-    ("give", 0, 0),
-    ("give", 0, 1),
-    ("finish", 1, 1),
-    ("finish", 0, 0),
-    ("finish", 0, 1),
+ORDERS = (
+    (
+        ("near", 0),
+        ("pass_on", 0, 0),
+        ("spread", 1, 1),
+        ("spread", 2, 3),
+        ("pass_on", 0, 3),
+        ("spread", 3, 2),
+        ("pass_on", 0, 1),
+        ("pass_on", 0, 2),
+        ("spread", 1, 0),
+        ("spread", 1, 2),
+        ("spread", 1, 3),
+        ("far", 0),
+        ("spread", 2, 2),
+        ("spread", 2, 0),
+        ("spread", 2, 1),
+        ("pass_on", 2, 2),
+        ("give", 0, 1),
+        ("spread", 3, 0),
+        ("pass_on", 1, 1),
+        ("pass_on", 2, 3),
+        ("pass_on", 2, 1),
+        ("pass_on", 2, 0),
+        ("spread", 3, 1),
+        ("spread", 3, 3),
+        ("far", 2),
+        ("give", 2, 0),
+        ("pass_on", 1, 0),
+        ("give", 0, 0),
+        ("pass_on", 3, 0),
+        ("pass_on", 1, 2),
+        ("pass_on", 3, 1),
+        ("pass_on", 3, 2),
+        ("pass_on", 1, 3),
+        ("give", 2, 1),
+        ("near", 2),
+        ("pass_on", 3, 3),
+        ("give", 2, 2),
+        ("give", 2, 3),
+        ("finish", 2, 0),
+        ("far", 3),
+        ("finish", 2, 1),
+        ("give", 3, 0),
+        ("near", 3),
+        ("finish", 2, 2),
+        ("give", 3, 2),
+        ("give", 3, 3),
+        ("finish", 0, 1),
+        ("finish", 2, 3),
+        ("far", 1),
+        ("finish", 3, 0),
+        ("give", 3, 1),
+        ("give", 1, 0),
+        ("give", 1, 2),
+        ("give", 1, 3),
+        ("finish", 3, 2),
+        ("give", 1, 1),
+        ("give", 0, 3),
+        ("finish", 0, 0),
+        ("finish", 3, 3),
+        ("near", 1),
+        ("give", 0, 2),
+        ("finish", 3, 1),
+        ("finish", 1, 0),
+        ("finish", 1, 2),
+        ("finish", 1, 3),
+        ("finish", 1, 1),
+        ("finish", 0, 3),
+        ("finish", 0, 2),
+    ),
+    (
+        ("near", 0),
+        ("spread", 3, 1),
+        ("spread", 2, 1),
+        ("pass_on", 0, 2),
+        ("pass_on", 0, 0),
+        ("pass_on", 0, 3),
+        ("pass_on", 0, 1),
+        ("spread", 3, 0),
+        ("spread", 2, 2),
+        ("spread", 2, 3),
+        ("spread", 2, 0),
+        ("far", 0),
+        ("pass_on", 2, 1),
+        ("pass_on", 2, 3),
+        ("spread", 1, 1),
+        ("pass_on", 2, 2),
+        ("pass_on", 3, 1),
+        ("pass_on", 3, 0),
+        ("pass_on", 2, 0),
+        ("spread", 1, 3),
+        ("spread", 3, 3),
+        ("far", 2),
+        ("spread", 3, 2),
+        ("give", 2, 1),
+        ("give", 2, 0),
+        ("give", 2, 3),
+        ("give", 2, 2),
+        ("near", 2),
+        ("pass_on", 1, 1),
+        ("finish", 2, 1),
+        ("spread", 1, 0),
+        ("finish", 2, 0),
+        ("pass_on", 3, 3),
+        ("spread", 1, 2),
+        ("pass_on", 3, 2),
+        ("finish", 2, 3),
+        ("far", 3),
+        ("give", 0, 1),
+        ("finish", 2, 2),
+        ("pass_on", 1, 0),
+        ("give", 3, 2),
+        ("give", 0, 0),
+        ("give", 3, 1),
+        ("give", 3, 3),
+        ("give", 3, 0),
+        ("pass_on", 1, 2),
+        ("pass_on", 1, 3),
+        ("near", 3),
+        ("far", 1),
+        ("give", 1, 0),
+        ("near", 1),
+        ("finish", 3, 2),
+        ("finish", 0, 1),
+        ("give", 1, 3),
+        ("give", 1, 2),
+        ("finish", 3, 0),
+        ("give", 1, 1),
+        ("finish", 0, 0),
+        ("finish", 3, 3),
+        ("give", 0, 3),
+        ("finish", 1, 0),
+        ("finish", 1, 3),
+        ("finish", 3, 1),
+        ("finish", 1, 2),
+        ("give", 0, 2),
+        ("finish", 1, 1),
+        ("finish", 0, 3),
+        ("finish", 0, 2),
+    ),
 )
 
 
@@ -67,6 +195,26 @@
     return total
 
 
+def mark(order):
+    seen, steps = set(), []
+    for step in order:
+        if step[0] == "finish":
+            step = step + (step[1] not in seen,)
+            seen.add(step[1])
+        steps.append(step)
+    return steps
+
+
+def segments(order):
+    parts = [[]]
+    for step in mark(order)[:-1]:
+        if step[0] in ("far", "near"):
+            parts += [[step], []]
+        else:
+            parts[-1].append(step)
+    return parts
+
+
 def kernel(
     experts, cap,
     tok_hbm, gain_hbm, ids_hbm, weight_hbm, gate_ref, up_ref, down_ref,
@@ -74,7 +222,7 @@
     tok_ref, gain_ref, ids_ref, weight_ref, norm, names, ranks, sides, picks, xs, xa, hid, po, rd, cx, rx, fo, ret, wgu, wd,
     in_sem, wgu_sem, wd_sem,
     z_send, z_recv, x_send, x_recv, d_send, d_recv, e_send, e_recv,
-    r_send, r_recv, v_send, v_recv, w_send, w_recv,
+    r_send, r_recv, n_recv, v_send, v_recv, w_send, w_recv,
 ):
     ep, c = lax.axis_index("ep"), lax.axis_index("tp")
     p, h = ep // 2, ep % 2
@@ -170,11 +318,13 @@
         first = 4 * mix_index(p, k, experts) + 2 * half
         return remote(xa.at[first + c], xa.at[first + 1 - c], send, recv.at[k], beside)
 
-    def r_copy(k, half, g):
-        n = 2 * (PIECES * k + g) + half
-        return remote(
-            cut(po, 4 * k + 2 * half + 1 - c, g), cut(rd, 2 * k + half, g),
-            r_send, r_recv.at[n], beside)
+    def r_copy(k, g, own):
+        half = h if own else 1 - h
+        recv = n_recv.at[k] if own else r_recv.at[PIECES * k + g]
+        return remote(cut(po, 4 * k + 2 * half + 1 - c, g), cut(rd, 2 * k + half, g), r_send, recv, beside)
+
+    def n_land(k):
+        return remote(po.at[4 * k + 2 * h + 1 - c], rd.at[2 * k + h], r_send, n_recv.at[k], beside)
 
     def v_copy(k, g):
         n = PIECES * k + g
@@ -228,7 +378,8 @@
 
     step = 2 * LANE
 
-    def compute(k, half):
+    def compute(k, own):
+        half = h if own else 1 - h
         rows = xa[pl.ds(4 * mix_index(p, k, experts) + 2 * half, 2)].reshape(2 * cap, width)
         for j in range(tiles):
             both = jnp.dot(rows, wgu[j], preferred_element_type=jnp.float32)
@@ -240,7 +391,7 @@
                 part = jnp.dot(hid[...], wd[:, n * step:(n + 1) * step], preferred_element_type=jnp.float32)
                 po[pl.ds(4 * k + 2 * half, 2), :, n * step:(n + 1) * step] = part.astype(
                     jnp.bfloat16).reshape(2, cap, step)
-            r_copy(k, half, g).start()
+            r_copy(k, g, own).start()
 
     def add(first, second):
         return (first.astype(jnp.float32) + second.astype(jnp.float32)).astype(jnp.bfloat16)
@@ -256,23 +407,25 @@
 
     def far(k):
         landing(k, 1 - h, e_send, e_recv).wait_recv()
-        compute(k, 1 - h)
+        compute(k, False)
 
     def near(k):
         landing(k, h, d_send, d_recv).wait_recv()
-        compute(k, h)
+        compute(k, True)
 
     def joined(k, half, g):
         cols = pl.ds(g * part_width, part_width)
-        r_copy(k, half, g).wait_recv()
         return add(po[4 * k + 2 * half + c, :, cols], rd[2 * k + half, :, cols])
 
     def give(k, g):
+        r_copy(k, g, False).wait_recv()
         cx[k, :, g * part_width:(g + 1) * part_width] = joined(k, 1 - h, g)
         v_copy(k, g).start()
 
-    def finish(k, g):
+    def finish(k, g, first):
         cols = pl.ds(g * part_width, part_width)
+        if first:
+            n_land(k).wait_recv()
         here = joined(k, h, g)
         v_copy(k, g).wait_recv()
         total = add(here, rx[k, :, cols])
@@ -318,15 +471,24 @@
 
     events = dict(spread=spread, pass_on=pass_on, far=far, near=near, give=give, finish=finish)
     if experts == len(TURNS[0]):
-        for name, s, *g in ORDER[:-1]:
-            events[name](turn(s), *g)
+        def run(steps, place):
+            for name, s, *rest in steps:
+                events[name](place(s), *rest)
+
+        for n, (outside, inside) in enumerate(zip(*map(segments, ORDERS))):
+            if outside == inside:
+                run(outside, turn)
+            else:
+                for side, steps in enumerate((outside, inside)):
+                    @pl.when(inner == side)
+                    def _():
+                        run(steps, lambda s: TURNS[side][s])
         settle()
-        for name, s, *g in ORDER[-1:]:
-            events[name](turn(s), *g)
+        run([mark(ORDERS[0])[-1]], turn)
     else:
         def each(event, k):
             for g in range(PIECES):
-                event(k, g)
+                event(k, g, *([g == 0] if event is finish else []))
 
         def stage(k, carry):
             near(k)
@@ -407,7 +569,7 @@
             dma((4,)), dma, dma,
             dma, dma((PIECES * (experts - 1),)), dma, dma((PIECES * experts,)),
             dma, dma((experts,)), dma, dma((experts,)),
-            dma, dma((2 * PIECES * experts,)), dma, dma((PIECES * experts,)), dma, dma((PIECES,)),
+            dma, dma((PIECES * experts,)), dma((experts,)), dma, dma((PIECES * experts,)), dma, dma((PIECES,)),
         ],
         compiler_params=pltpu.CompilerParams(
             collective_id=0, has_side_effects=True, vmem_limit_bytes=60 * 1024 * 1024),

time: 69.7 us -> 67.4 us (0.967)
  Pallas kernels: 68.7 us -> 66.4 us
    pallas_call x1, Pallas kernels: 68.7 us -> 66.4 us  [local(): pl.pallas_call(functools.partial(kernel, experts, cap), out_shape=pltpu.V...]
where the time goes in v4:
time: 67.4 us; the launch traced here: 67.2 us
  Pallas kernels  66.4 us (99%)
  local copies, waits for them, and re-layouts  0.8 us (1%)
    pallas_call x1, Pallas kernels, local(): pl.pallas_call(functools.partial(kernel, experts, cap), out_shape=pltpu.V...  66.4 us

profile of v4, /device:TPU:8, one launch (start us, length us, event | category | flops | bytes accessed | tf_op | source)
XLA Modules:
  0.0 67.2 jit_solution(2183372619002701349)
XLA Ops:
  0.0 66.4 %shard_map.73 = bf16[128,2048]{1,0:T(8,128)(2,1)S(1)} custom-call(bf16[128,2048]{1,0:T(8,128)(2,1)} %tok_hbm.1, f32[1,2048]{1,0:T(1,128)} %bitcast.3, s32[2,128]{1,0:T(2,128)} %bitcast.4, f32[2,128]{1,0:T(2,128)} %bitcast.5, bf16[2048,896]{1,0:T(8,128)(2,1)} %gate_ref.1, bf16[2048,896]{1,0:T(8,128)(2,1)} %up_ref.1, bf16[896,2048]{1,0:T(8,128)(2,1)} %down_ref.1), custom_call_target="tpu_custom_call" | custom-call | tf_op jit(solution)/shard_map/pallas_call | solution.py:543
  66.4 0.8 %copy.9 = bf16[128,2048]{1,0:T(8,128)(2,1)} copy(bf16[128,2048]{1,0:T(8,128)(2,1)S(1)} %shard_map.73) | data formatting | bytes 1048576

commit v5 on v4

--- a/solution.py
+++ b/solution.py
@@ -351,16 +351,18 @@
         outside, inside = TURNS[0][s], TURNS[1][s]
         return outside if outside == inside else outside + inner * (inside - outside)
 
+    xa[4 * p + 2 * h + c] = picked(p)
+    if experts == len(TURNS[0]):
+        for k in range(1, experts):
+            xs[mix_index(p, k, experts)] = picked(mix_index(p, k, experts))
+
     pl.semaphore_wait(barrier, experts + 1)
 
-    xa[4 * p + 2 * h + c] = picked(p)
     for g in range(PIECES):
         x_copy(0, g).start()
         d_copy(0, g).start()
 
     if experts == len(TURNS[0]):
-        for k in range(1, experts):
-            xs[mix_index(p, k, experts)] = picked(mix_index(p, k, experts))
         for side, sends in enumerate(SENDS):
             @pl.when(inner == side)
             def _():

time: 67.4 us -> 67 us (level)
  no operation moved by 1% of the time
where the time goes in v5:
time: 67 us; the launch traced here: 66.9 us
  Pallas kernels  66.1 us (99%)
  local copies, waits for them, and re-layouts  0.8 us (1%)
    pallas_call x1, Pallas kernels, local(): pl.pallas_call(functools.partial(kernel, experts, cap), out_shape=pltpu.V...  66.1 us

profile of v5, /device:TPU:8, one launch (start us, length us, event | category | flops | bytes accessed | tf_op | source)
XLA Modules:
  0.0 66.9 jit_solution(14394967953169927440)
XLA Ops:
  0.0 66.1 %shard_map.73 = bf16[128,2048]{1,0:T(8,128)(2,1)S(1)} custom-call(bf16[128,2048]{1,0:T(8,128)(2,1)} %tok_hbm.1, f32[1,2048]{1,0:T(1,128)} %bitcast.3, s32[2,128]{1,0:T(2,128)} %bitcast.4, f32[2,128]{1,0:T(2,128)} %bitcast.5, bf16[2048,896]{1,0:T(8,128)(2,1)} %gate_ref.1, bf16[2048,896]{1,0:T(8,128)(2,1)} %up_ref.1, bf16[896,2048]{1,0:T(8,128)(2,1)} %down_ref.1), custom_call_target="tpu_custom_call" | custom-call | tf_op jit(solution)/shard_map/pallas_call | solution.py:545
  66.1 0.8 %copy.9 = bf16[128,2048]{1,0:T(8,128)(2,1)} copy(bf16[128,2048]{1,0:T(8,128)(2,1)S(1)} %shard_map.73) | data formatting | bytes 1048576
